TPU v7x, 32 devices: a whole 2x2x4 slice. The times are simulated.
32 devices in a mesh: grp: 2 (over y), sp: 4 (over z), tp: 4 (over x, core).
Axes of the slice: x: 2, y: 2, z: 4, core: 2. Of those that a mesh axis runs over, the one named last changes fastest.
Arguments:
- queries: bfloat16 [4096, 1024], P(('grp', 'sp'), 'tp'), parts along dimension 0, may hold values from -6 to 6
- memory_keys: bfloat16 [4096, 1024], P(('grp', 'sp'), 'tp'), parts along dimension 0, may hold values from -6 to 6
- memory_values: bfloat16 [4096, 1024], P(('grp', 'sp'), 'tp'), parts along dimension 0, may hold values from -6 to 6
- output_preactivation: bfloat16 [4096, 1024], P(('grp', 'sp'), 'tp'), parts along dimension 0, may hold values from -12 to 12
- input_preactivation: float32 [8, 4096], P('tp', ('grp', 'sp')), parts along dimension 1, may hold values from -6 to 140
- forget_preactivation: float32 [8, 4096], P('tp', ('grp', 'sp')), parts along dimension 1, as said below
- extra_forget_terms: float32 [8, 4096], P('tp', ('grp', 'sp')), parts along dimension 1, may hold values from -1 to 0, as said below
- head_norm_gain: float32 [128], replicated, may hold values from 0.1 to 1.9
- output_projection_matrix: bfloat16 [1024, 2048], P('tp'), may hold values from -0.1875 to 0.1875
- residual: bfloat16 [4096, 2048], P(('grp', 'sp', 'tp')), parts along dimension 0, may hold values from -6 to 6
- feedforward_norm_gain: float32 [2048], replicated, may hold values from 0.1 to 1.9
- feedforward_up_matrix: bfloat16 [2048, 8192], P('sp', 'tp'), may hold values from -0.125 to 0.125
- feedforward_down_matrix: bfloat16 [8192, 2048], P('tp', 'sp'), may hold values from -0.0625 to 0.0625
Outputs:
- layer_out: bfloat16 [4096, 2048], P(('grp', 'sp', 'tp')), parts along dimension 0
There are 2 independent parts, one for each index of `grp`. A program takes and returns all parts, laid end to end along the dimension named above; an argument that names none is the same for every part. Nothing has to cross between parts.
Inputs may be any that keep to these rules, and one draw needn't show every extreme that they name: `forget_preactivation`: forget gate pre-activations. `extra_forget_terms`: extra log forget terms, zero at most positions.
All inputs are finite; a program needn't handle non-finite values.
Results may differ from a plain program's by a relative error of at most 0.018.
Values may be sent and summed in bfloat16 or wider, within the bound.
A program may use at most 64 MiB of HBM per device.

v0:
```python
import jax
import jax.numpy as jnp
from jax import lax
from jax.sharding import PartitionSpec as P

BLOCK = 128
neg_big = -1e30
norm_eps = 1e-06
highest = lax.Precision.HIGHEST


def entering(x, axis, combine, identity):
    length, position = (lax.axis_size(axis), lax.axis_index(axis))
    everything = jax.tree.map(lambda part: lax.all_gather(part, axis), x)
    start = jax.tree.map(
        lambda part, zero: jnp.broadcast_to(jnp.asarray(zero, part.dtype), part.shape), x, identity
    )

    def step(k, before):
        reached = k < position
        new = combine(before, jax.tree.map(lambda part: part[k], everything))
        return jax.tree.map(lambda a, b: jnp.where(reached, a, b), new, before)

    return lax.fori_loop(0, length, step, start)


def rms_norm(tensor, gain_vec):
    mean_sq = jnp.mean(tensor * tensor, axis=-1, keepdims=True)
    return tensor * lax.rsqrt(mean_sq + norm_eps) * gain_vec


def combine(earlier, later):
    total_e, max_e, memory_e = earlier
    total_l, max_l, memory_l = later
    carried = total_l + max_e
    new_max = jnp.maximum(carried, max_l)
    old_part = jnp.exp(carried - new_max)
    new_part = jnp.exp(max_l - new_max)
    return (
        total_e + total_l,
        new_max,
        old_part[..., None, None] * memory_e + new_part[..., None, None] * memory_l,
    )


def block_summary(key_blk, val_blk, gate_blk, decay_logarithm):
    block_total = decay_logarithm[..., -1]
    tail_log = block_total[..., None] - decay_logarithm + gate_blk
    tail_max = jnp.max(tail_log, axis=-1)
    weights = jnp.exp(tail_log - tail_max[..., None])
    memory = jnp.einsum("bhsv,bhsk->bhvk", weights[..., None] * val_blk, key_blk, precision=highest)
    return (block_total, tail_max, memory)


def shards(
    queries,
    memory_keys,
    memory_values,
    output_preactivation,
    input_preactivation,
    forget_preactivation,
    extra_forget_terms,
    head_norm_gain,
    output_projection_matrix,
    residual,
    feedforward_norm_gain,
    feedforward_up_matrix,
    feedforward_down_matrix,
):
    tok_count = queries.shape[0]
    head_count = input_preactivation.shape[0]
    head_dim = queries.shape[1] // head_count
    block_len = BLOCK
    block_count = tok_count // block_len

    def to_blocks(tensor):
        return (
            tensor.astype(jnp.float32)
            .reshape(block_count, block_len, head_count, head_dim)
            .transpose(0, 2, 1, 3)
        )

    def gate_block_list(tensor):
        return tensor.reshape(head_count, block_count, block_len).transpose(1, 0, 2)

    query_blk = to_blocks(queries)
    key_blk = to_blocks(memory_keys) * head_dim ** (-0.5)
    val_blk = to_blocks(memory_values)
    gate_blk = gate_block_list(input_preactivation)
    decay_logarithm = jnp.cumsum(
        gate_block_list(jax.nn.log_sigmoid(forget_preactivation) + extra_forget_terms), axis=-1
    )
    summaries = block_summary(key_blk, val_blk, gate_blk, decay_logarithm)
    zero_heads = jnp.zeros((head_count,), jnp.float32)
    zero_memory = jnp.zeros((head_count, head_dim, head_dim), jnp.float32)
    zero_state = (zero_heads, jnp.full((head_count,), neg_big, jnp.float32), zero_memory)
    prefixes = []
    running = zero_state
    for block_idx in range(block_count):
        prefixes.append(running)
        running = combine(running, tuple((member[block_idx] for member in summaries)))
    before = entering(running, "sp", combine, zero_state)
    anchor = (zero_heads, zero_heads, zero_memory)
    incoming = combine(anchor, before)
    starts = [combine(incoming, prefix) for prefix in prefixes]
    start_max = jnp.stack([each_state[1] for each_state in starts])
    start_memory = jnp.stack([each_state[2] for each_state in starts])
    causal = lax.broadcasted_iota(jnp.int32, (block_len, block_len), 0) >= lax.broadcasted_iota(
        jnp.int32, (block_len, block_len), 1
    )
    log_weight = (
        decay_logarithm[..., :, None] - decay_logarithm[..., None, :] + gate_blk[..., None, :]
    )
    log_weight = jnp.where(causal, log_weight, neg_big)
    carry_log = decay_logarithm + start_max[..., None]
    row_max = jnp.maximum(jnp.max(log_weight, axis=-1), carry_log)
    scores = jnp.einsum("bhtd,bhsd->bhts", query_blk, key_blk, precision=highest) * jnp.exp(
        log_weight - row_max[..., None]
    )
    carry_scale = jnp.exp(carry_log - row_max)
    hidden = jnp.einsum("bhts,bhsv->bhtv", scores, val_blk, precision=highest)
    hidden = hidden + carry_scale[..., None] * jnp.einsum(
        "bhvk,bhtk->bhtv", start_memory, query_blk, precision=highest
    )
    hidden = hidden.transpose(0, 2, 1, 3).reshape(tok_count, head_count, head_dim)
    gated = rms_norm(hidden, head_norm_gain) * jax.nn.sigmoid(
        output_preactivation.astype(jnp.float32).reshape(tok_count, head_count, head_dim)
    )
    mixed = gated.reshape(tok_count, head_count * head_dim).astype(jnp.bfloat16)
    branch = lax.psum_scatter(
        jnp.dot(mixed, output_projection_matrix, preferred_element_type=jnp.float32).astype(
            jnp.bfloat16
        ),
        "tp",
        scatter_dimension=0,
        tiled=True,
    ).astype(jnp.float32)
    mid_state = (residual.astype(jnp.float32) + branch).astype(jnp.bfloat16)
    normed = rms_norm(mid_state.astype(jnp.float32), feedforward_norm_gain).astype(jnp.bfloat16)
    normed_all = lax.all_gather(normed, "tp", axis=0, tiled=True)
    upward = jnp.dot(
        normed_all,
        lax.all_gather(feedforward_up_matrix, "sp", axis=0, tiled=True),
        preferred_element_type=jnp.float32,
    )
    active = jnp.square(jax.nn.relu(upward)).astype(jnp.bfloat16)
    mlp_terms = jnp.dot(
        active,
        lax.all_gather(feedforward_down_matrix, "sp", axis=1, tiled=True),
        preferred_element_type=jnp.float32,
    )
    mlp_sum = lax.psum_scatter(
        mlp_terms.astype(jnp.bfloat16), "tp", scatter_dimension=0, tiled=True
    ).astype(jnp.float32)
    return (mid_state.astype(jnp.float32) + mlp_sum).astype(jnp.bfloat16)


def solution(mesh):
    in_specs = (
        P(("grp", "sp"), "tp"),
        P(("grp", "sp"), "tp"),
        P(("grp", "sp"), "tp"),
        P(("grp", "sp"), "tp"),
        P("tp", ("grp", "sp")),
        P("tp", ("grp", "sp")),
        P("tp", ("grp", "sp")),
        P(),
        P("tp", None),
        P(("grp", "sp", "tp"), None),
        P(),
        P("sp", "tp"),
        P("tp", "sp"),
    )
    out_specs = P(("grp", "sp", "tp"), None)
    return jax.shard_map(shards, mesh=mesh, in_specs=in_specs, out_specs=out_specs, check_vma=False)
```

profile of v0, /device:TPU:0, one launch (start us, length us, event | category | flops | bytes accessed | tf_op | source)
XLA Modules:
  0.0 468.9 jit_solution(10719103995341335332)
XLA Ops:
  6.6 0.8 fusion.50
  7.4 1.2 reduce_window_sum.11
  9.1 0.9 fusion.65
  10.0 0.8 subtract_exponential_fusion.2
  10.8 12.6 %all-gather.1 = f32[4,1,2]{2,1,0:T(1,128)S(1)} all-gather(f32[1,1,2]{2,1,0:T(1,128)S(1)} %get-tuple-element.255), channel_id=1, replica_groups=mesh['grp'=2,'sp'=4,'tp'=4] {'sp'}, dimensions={0}, use_global_device_ids=true | all-gather | bytes 40 | tf_op jit(solution)/shard_map/all_gather | solution.py:14
  23.5 7.6 %all-gather = f32[4,1,2]{2,1,0:T(1,128)S(1)} all-gather(f32[1,1,2]{2,1,0:T(1,128)S(1)} %get-tuple-element.256), channel_id=1, replica_groups=mesh['grp'=2,'sp'=4,'tp'=4] {'sp'}, dimensions={0}, use_global_device_ids=true | all-gather | bytes 40 | tf_op jit(solution)/shard_map/all_gather | solution.py:14
  31.0 1.0 reshape.306
  32.2 1.0 convert_multiply_fusion.2
  33.5 0.7 fusion.22
  34.4 15.0 %all_gather.23 = f32[4,2,128,128]{3,2,1,0:T(8,128)S(1)} all-gather(f32[1,2,128,128]{3,2,1,0:T(8,128)S(1)} %fusion.40), channel_id=1, replica_groups=mesh['grp'=2,'sp'=4,'tp'=4] {'sp'}, dimensions={0}, use_global_device_ids=true | all-gather | bytes 655360 | tf_op jit(solution)/shard_map/all_gather | solution.py:14
  49.4 0.6 while.18
  50.7 0.7 fusion.5
  51.7 0.7 fusion.7
  53.9 2.1 convolution_convert_fusion
  56.1 31.6 %reduce-scatter.3.cloned.1.call-done = bf16[128,2048]{1,0:T(8,128)(2,1)} async-done(((bf16[512,2048]{1,0:T(8,128)(2,1)}), bf16[128,2048]{1,0:T(8,128)(2,1)}) %reduce-scatter.3.cloned.1.call-update) | async-done | bytes 524304 | tf_op jit(solution)/shard_map/reduce_scatter | solution.py:130
  87.6 1.3 fusion.8
  89.0 2.0 fusion.10
  91.1 0.7 all-gather.8.cloned.1.call-update
  92.6 21.2 %all-gather.6.cloned.1.call-done = bf16[512,2048]{1,0:T(8,128)(2,1)} async-done(((bf16[128,2048]{1,0:T(8,128)(2,1)}), bf16[512,2048]{1,0:T(8,128)(2,1)}) %all-gather.6.cloned.1.call-update) | async-done | bytes 2097168 | tf_op jit(solution)/shard_map/all_gather | solution.py:140
  113.8 151.2 %all-gather.8.cloned.1.call-done = bf16[2048,2048]{1,0:T(8,128)(2,1)} async-done(((bf16[512,2048]{1,0:T(8,128)(2,1)}), bf16[2048,2048]{1,0:T(8,128)(2,1)}) %all-gather.8.cloned.1.call-update) | async-done | bytes 8388624 | tf_op jit(solution)/shard_map/all_gather | solution.py:143
  265.0 149.3 %all-gather.10.cloned.1.call-done = bf16[2048,2048]{1,0:T(8,128)(2,1)} async-done(((bf16[2048,512]{1,0:T(8,128)(2,1)}), bf16[2048,2048]{1,0:T(8,128)(2,1)}) %all-gather.10.cloned.1.call-update) | async-done | bytes 8388624 | tf_op jit(solution)/shard_map/all_gather | solution.py:149
  414.2 16.5 %convolution_convert_fusion.1 = bf16[512,2048]{1,0:T(8,128)(2,1)} fusion(bf16[2048,2048]{1,0:T(8,128)(2,1)} %all-gather.10.cloned.1.call-done, bf16[512,2048]{1,0:T(8,128)(2,1)} %all-gather.6.cloned.1.call-done, bf16[2048,2048]{1,0:T(8,128)(2,1)} %all-gather.8.cloned.1.call-done), kind=kOutput, calls=%fused_computation.16 | convolution fusion | flops 8594128896 | bytes 20971520 | tf_op jit(solution)/shard_map/dot_general | solution.py:147
  430.8 29.5 %reduce-scatter.5.cloned.1.call-done = bf16[128,2048]{1,0:T(8,128)(2,1)} async-done(((bf16[512,2048]{1,0:T(8,128)(2,1)}), bf16[128,2048]{1,0:T(8,128)(2,1)}) %reduce-scatter.5.cloned.1.call-update) | async-done | bytes 524304 | tf_op jit(solution)/shard_map/reduce_scatter | solution.py:152
  460.3 2.1 fusion.11
  (68 shorter events, 5.0 us)
Async XLA Ops:
  6.5 47.3 %copy-start = (bf16[256,2048]{1,0:T(8,128)(2,1)S(1)}, bf16[256,2048]{1,0:T(8,128)(2,1)}, u32[]{:S(2)}) copy-start(bf16[256,2048]{1,0:T(8,128)(2,1)} %param.23) | copy-start | bytes 3145732
  6.5 43.5 %copy-start.4 = (f32[2,512]{1,0:T(2,128)S(1)}, f32[2,512]{1,0:T(2,128)}, u32[]{:S(2)}) copy-start(f32[2,512]{1,0:T(2,128)} %param.19) | copy-start | bytes 12292
  6.5 44.1 %copy-start.7 = (f32[128]{0:T(128)S(1)}, f32[128]{0:T(128)}, u32[]{:S(2)}) copy-start(f32[128]{0:T(128)} %param.22) | copy-start | bytes 1540
  6.5 44.1 %copy-start.3 = (bf16[512,256]{1,0:T(8,128)(2,1)S(1)}, bf16[512,256]{1,0:T(8,128)(2,1)}, u32[]{:S(2)}) copy-start(bf16[512,256]{1,0:T(8,128)(2,1)} %param.15) | copy-start | bytes 786436
  6.5 81.1 %reduce-scatter.3.cloned.1.call-start = ((), (), s32[]{:S(2)}) async-start(), calls=%async_computation.2 | async-start | bytes 2621440 | tf_op jit(solution)/shard_map/reduce_scatter | solution.py:130
  50.7 3.2 copy-start.6
  53.0 34.7 %copy-start.1 = (bf16[128,2048]{1,0:T(8,128)(2,1)S(1)}, bf16[128,2048]{1,0:T(8,128)(2,1)}, u32[]{:S(2)}) copy-start(bf16[128,2048]{1,0:T(8,128)(2,1)} %param.24) | copy-start | bytes 1572868
  53.9 35.1 %copy-start.5 = (f32[2048]{0:T(1024)S(1)}, f32[2048]{0:T(1024)}, u32[]{:S(2)}) copy-start(f32[2048]{0:T(1024)} %param.25) | copy-start | bytes 24580
  56.0 57.7 %all-gather.6.cloned.1.call-start = ((), (), s32[]{:S(2)}) async-start(), calls=%async_computation.3 | async-start | bytes 2621440 | tf_op jit(solution)/shard_map/all_gather | solution.py:140
  91.0 174.0 %all-gather.8.cloned.1.call-start = ((), (), s32[]{:S(2)}) async-start(), calls=%async_computation.4 | async-start | bytes 10485760 | tf_op jit(solution)/shard_map/all_gather | solution.py:143
  91.8 322.5 %all-gather.10.cloned.1.call-start = ((), (), s32[]{:S(2)}) async-start(), calls=%async_computation.5 | async-start | bytes 10485760 | tf_op jit(solution)/shard_map/all_gather | solution.py:149
  92.3 368.0 %copy-start.2 = (bf16[128,2048]{1,0:T(8,128)(2,1)S(1)}, bf16[128,2048]{1,0:T(8,128)(2,1)}, u32[]{:S(2)}) copy-start(bf16[128,2048]{1,0:T(8,128)(2,1)} %reduce-scatter.3.cloned.1.call-done) | copy-start | bytes 1572868
  92.3 367.9 %reduce-scatter.5.cloned.1.call-start = ((), (), s32[]{:S(2)}) async-start(), calls=%async_computation.6 | async-start | bytes 2621440 | tf_op jit(solution)/shard_map/reduce_scatter | solution.py:152
Sparse Core Ops, SparseCore 0:
  56.1 31.4 reduce-scatter.2
  91.1 22.5 all-gather.5
  115.3 149.6 all-gather.7
  266.4 147.7 all-gather.9
  430.9 29.3 reduce-scatter.4
where the time goes:
time: 469 us
  waiting for transfers between devices  384 us (82%)
  blocking collectives  35.2 us (8%)
  matrix products  21.1 us (4%)
  between operations  13.4 us (3%)
  other arithmetic  11.6 us (2%)
    all_gather x1, waiting for transfers between devices, shards(): lax.all_gather(feedforward_up_matrix, 'sp', axis=0, tiled=True)  151 us
    all_gather x1, waiting for transfers between devices, shards(): lax.all_gather(feedforward_down_matrix, 'sp', axis=1, tiled=True)  149 us
    all_gather x3, blocking collectives, entering(): everything = jax.tree.map(lambda part: lax.all_gather(part, axis), x)  35.2 us
    reduce_scatter x1, waiting for transfers between devices, shards(): lax.psum_scatter(jnp.dot(mixed, output_projection_matrix, preferred_eleme...  31.6 us
    reduce_scatter x1, waiting for transfers between devices, shards(): lax.psum_scatter(mlp_terms.astype(jnp.bfloat16), 'tp', scatter_dimension=...  29.5 us
    all_gather x1, waiting for transfers between devices, shards(): normed_all = lax.all_gather(normed, 'tp', axis=0, tiled=True)  21.2 us
    dot_general x1, matrix products, shards(): jnp.dot(active, lax.all_gather(feedforward_down_matrix, 'sp', axis=1, til...  16.5 us
  transfers between devices with their start and end apart: 5, of which 5 were waited for; matrix products, arithmetic and copies ran while one was open for 0% of the time, Pallas kernels for 0%

commit v1 on v0

--- a/solution.py
+++ b/solution.py
@@ -146,7 +146,10 @@
     active = jnp.square(jax.nn.relu(upward)).astype(jnp.bfloat16)
     mlp_terms = jnp.dot(
         active,
-        lax.all_gather(feedforward_down_matrix, "sp", axis=1, tiled=True),
+        jnp.concatenate(
+            lax.all_to_all(jnp.stack([feedforward_down_matrix] * lax.axis_size("sp")), "sp", 0, 0),
+            axis=1,
+        ),
         preferred_element_type=jnp.float32,
     )
     mlp_sum = lax.psum_scatter(

time: 469 us -> 478 us (1.019)
  local copies, waits for them, and re-layouts: 3.07 us -> 10.3 us
  waiting for transfers between devices: 384 us -> 378 us
  starting transfers between devices: 0.37 us -> 5.94 us
    all_to_all x0 -> x1, waiting for transfers between devices: none -> 308 us  [shards(): lax.all_to_all(jnp.stack([feedforward_down_matrix] * lax.axis_size('sp'))...]
    all_gather x1, waiting for transfers between devices: 151 us -> 0.01 us  [shards(): lax.all_gather(feedforward_up_matrix, 'sp', axis=0, tiled=True)]
    all_gather x1 -> x0, waiting for transfers between devices: 149 us -> none  [shards(): lax.all_gather(feedforward_down_matrix, 'sp', axis=1, tiled=True)]
    all_gather x1, waiting for transfers between devices: 21.2 us -> 8.89 us  [shards(): normed_all = lax.all_gather(normed, 'tp', axis=0, tiled=True)]
    all_to_all x0 -> x1, starting transfers between devices: none -> 5.63 us  [shards(): lax.all_to_all(jnp.stack([feedforward_down_matrix] * lax.axis_size('sp'))...]
  transfers between devices with their start and end apart: 5 -> 5, of which waited for: 5 -> 4; matrix products, arithmetic and copies ran while one was open for 0% -> 2% of each run, Pallas kernels for 0% -> 0%
where the time goes in v1:
time: 478 us
  waiting for transfers between devices  378 us (79%)
  blocking collectives  36.6 us (8%)
  matrix products  21.2 us (4%)
  between operations  13.4 us (3%)
  other arithmetic  11.6 us (2%)
  local copies, waits for them, and re-layouts  10.3 us (2%)
  starting transfers between devices  5.94 us (1%)
    all_to_all x1, waiting for transfers between devices, shards(): lax.all_to_all(jnp.stack([feedforward_down_matrix] * lax.axis_size('sp'))...  308 us
    all_gather x3, blocking collectives, entering(): everything = jax.tree.map(lambda part: lax.all_gather(part, axis), x)  36.6 us
    reduce_scatter x1, waiting for transfers between devices, shards(): lax.psum_scatter(jnp.dot(mixed, output_projection_matrix, preferred_eleme...  30.9 us
    reduce_scatter x1, waiting for transfers between devices, shards(): lax.psum_scatter(mlp_terms.astype(jnp.bfloat16), 'tp', scatter_dimension=...  29.7 us
    dot_general x1, matrix products, shards(): jnp.dot(active, jnp.concatenate(lax.all_to_all(jnp.stack([feedforward_dow...  16.6 us
  transfers between devices with their start and end apart: 5, of which 4 were waited for; matrix products, arithmetic and copies ran while one was open for 2% of the time, Pallas kernels for 0%

profile of v1, /device:TPU:0, one launch (start us, length us, event | category | flops | bytes accessed | tf_op | source)
XLA Modules:
  0.0 477.6 jit_solution(9126041023727417653)
XLA Ops:
  6.5 0.8 fusion.50
  7.4 1.2 reduce_window_sum.11
  9.1 0.8 fusion.65
  9.9 0.8 subtract_exponential_fusion.2
  10.8 1.0 convert_multiply_fusion.2
  12.1 1.0 reshape.314
  13.3 0.7 fusion.22
  14.1 17.4 %all_gather.20 = f32[4,2,128,128]{3,2,1,0:T(8,128)S(1)} all-gather(f32[1,2,128,128]{3,2,1,0:T(8,128)S(1)} %fusion.40), channel_id=1, replica_groups=mesh['grp'=2,'sp'=4,'tp'=4] {'sp'}, dimensions={0}, use_global_device_ids=true | all-gather | bytes 655360 | tf_op jit(solution)/shard_map/all_gather | solution.py:14
  31.5 11.7 %all-gather.1 = f32[4,1,2]{2,1,0:T(1,128)S(1)} all-gather(f32[1,1,2]{2,1,0:T(1,128)S(1)} %get-tuple-element.255), channel_id=1, replica_groups=mesh['grp'=2,'sp'=4,'tp'=4] {'sp'}, dimensions={0}, use_global_device_ids=true | all-gather | bytes 40 | tf_op jit(solution)/shard_map/all_gather | solution.py:14
  43.2 7.6 %all-gather = f32[4,1,2]{2,1,0:T(1,128)S(1)} all-gather(f32[1,1,2]{2,1,0:T(1,128)S(1)} %get-tuple-element.256), channel_id=1, replica_groups=mesh['grp'=2,'sp'=4,'tp'=4] {'sp'}, dimensions={0}, use_global_device_ids=true | all-gather | bytes 40 | tf_op jit(solution)/shard_map/all_gather | solution.py:14
  52.0 0.7 fusion.5
  55.2 2.1 convolution_convert_fusion
  57.4 30.9 %reduce-scatter.3.cloned.1.call-done = bf16[128,2048]{1,0:T(8,128)(2,1)} async-done(((bf16[512,2048]{1,0:T(8,128)(2,1)}), bf16[128,2048]{1,0:T(8,128)(2,1)}) %reduce-scatter.3.cloned.1.call-update) | async-done | bytes 524304 | tf_op jit(solution)/shard_map/reduce_scatter | solution.py:130
  88.3 1.3 fusion.8
  89.6 2.0 fusion.10
  91.7 2.9 copy.62
  94.7 4.3 stack.47
  98.9 5.6 %all-to-all-start = ((bf16[4,2048,512]{1,2,0:T(8,128)(2,1)}), bf16[4,2048,512]{1,2,0:T(8,128)(2,1)}, u32[]{:S(2)}, u32[]{:S(2)}) async-start(bf16[4,2048,512]{1,2,0:T(8,128)(2,1)} %stack.47), calls=%async_computation.1 | async-start | bytes 16777216 | tf_op jit(solution)/shard_map/all_to_all | solution.py:150
  104.6 0.7 all-gather.7.cloned.1.call-update
  105.5 8.9 %all-gather.5.cloned.1.call-done = bf16[512,2048]{1,0:T(8,128)(2,1)} async-done(((bf16[128,2048]{1,0:T(8,128)(2,1)}), bf16[512,2048]{1,0:T(8,128)(2,1)}) %all-gather.5.cloned.1.call-update) | async-done | bytes 2097168 | tf_op jit(solution)/shard_map/all_gather | solution.py:140
  114.4 308.2 %all-to-all-done = bf16[4,2048,512]{1,2,0:T(8,128)(2,1)} async-done(((bf16[4,2048,512]{1,2,0:T(8,128)(2,1)}), bf16[4,2048,512]{1,2,0:T(8,128)(2,1)}, u32[]{:S(2)}, u32[]{:S(2)}) %all-to-all-start) | async-done | bytes 8388640 | tf_op jit(solution)/shard_map/all_to_all | solution.py:150
  422.6 16.6 %convolution_convert_fusion.1 = bf16[512,2048]{1,0:T(8,128)(2,1)} fusion(bf16[2048,2048]{0,1:T(8,128)(2,1)} %bitcast.36, bf16[512,2048]{1,0:T(8,128)(2,1)} %all-gather.5.cloned.1.call-done, bf16[2048,2048]{1,0:T(8,128)(2,1)} %all-gather.7.cloned.1.call-done), kind=kOutput, calls=%fused_computation.16 | convolution fusion | flops 8594128896 | bytes 20971520 | tf_op jit(solution)/shard_map/dot_general | solution.py:147
  439.2 29.7 %reduce-scatter.5.cloned.1.call-done = bf16[128,2048]{1,0:T(8,128)(2,1)} async-done(((bf16[512,2048]{1,0:T(8,128)(2,1)}), bf16[128,2048]{1,0:T(8,128)(2,1)}) %reduce-scatter.5.cloned.1.call-update) | async-done | bytes 524304 | tf_op jit(solution)/shard_map/reduce_scatter | solution.py:155
  469.0 2.1 fusion.11
  (71 shorter events, 5.7 us)
Async XLA Ops:
  6.5 48.7 %copy-start = (bf16[256,2048]{1,0:T(8,128)(2,1)S(1)}, bf16[256,2048]{1,0:T(8,128)(2,1)}, u32[]{:S(2)}) copy-start(bf16[256,2048]{1,0:T(8,128)(2,1)} %param.23) | copy-start | bytes 3145732
  6.5 44.9 %copy-start.5 = (f32[2,512]{1,0:T(2,128)S(1)}, f32[2,512]{1,0:T(2,128)}, u32[]{:S(2)}) copy-start(f32[2,512]{1,0:T(2,128)} %param.19) | copy-start | bytes 12292
  6.5 45.4 %copy-start.4 = (bf16[512,256]{1,0:T(8,128)(2,1)S(1)}, bf16[512,256]{1,0:T(8,128)(2,1)}, u32[]{:S(2)}) copy-start(bf16[512,256]{1,0:T(8,128)(2,1)} %param.15) | copy-start | bytes 786436
  6.5 81.8 %reduce-scatter.3.cloned.1.call-start = ((), (), s32[]{:S(2)}) async-start(), calls=%async_computation.3 | async-start | bytes 2621440 | tf_op jit(solution)/shard_map/reduce_scatter | solution.py:130
  51.4 3.2 copy-start.8
  52.0 3.2 copy-start.7
  54.3 34.0 %copy-start.1 = (bf16[128,2048]{1,0:T(8,128)(2,1)S(1)}, bf16[128,2048]{1,0:T(8,128)(2,1)}, u32[]{:S(2)}) copy-start(bf16[128,2048]{1,0:T(8,128)(2,1)} %param.24) | copy-start | bytes 1572868
  55.2 34.4 %copy-start.6 = (f32[2048]{0:T(1024)S(1)}, f32[2048]{0:T(1024)}, u32[]{:S(2)}) copy-start(f32[2048]{0:T(1024)} %param.25) | copy-start | bytes 24580
  57.4 57.1 %all-gather.5.cloned.1.call-start = ((), (), s32[]{:S(2)}) async-start(), calls=%async_computation.4 | async-start | bytes 2621440 | tf_op jit(solution)/shard_map/all_gather | solution.py:140
  98.9 323.7 %all-to-all-start = ((bf16[4,2048,512]{1,2,0:T(8,128)(2,1)}), bf16[4,2048,512]{1,2,0:T(8,128)(2,1)}, u32[]{:S(2)}, u32[]{:S(2)}) async-start(bf16[4,2048,512]{1,2,0:T(8,128)(2,1)} %stack.47), calls=%async_computation.1 | async-start | bytes 16777216 | tf_op jit(solution)/shard_map/all_to_all | solution.py:150
  104.6 318.0 %all-gather.7.cloned.1.call-start = ((), (), s32[]{:S(2)}) async-start(), calls=%async_computation.5 | async-start | bytes 10485760 | tf_op jit(solution)/shard_map/all_gather | solution.py:143
  105.3 363.7 %reduce-scatter.5.cloned.1.call-start = ((), (), s32[]{:S(2)}) async-start(), calls=%async_computation.6 | async-start | bytes 2621440 | tf_op jit(solution)/shard_map/reduce_scatter | solution.py:155
  422.6 46.4 %copy-start.2 = (bf16[128,2048]{1,0:T(8,128)(2,1)S(1)}, bf16[128,2048]{1,0:T(8,128)(2,1)}, u32[]{:S(2)}) copy-start(bf16[128,2048]{1,0:T(8,128)(2,1)} %param.24) | copy-start | bytes 1572868
  422.6 46.4 %copy-start.3 = (bf16[128,2048]{1,0:T(8,128)(2,1)S(1)}, bf16[128,2048]{1,0:T(8,128)(2,1)}, u32[]{:S(2)}) copy-start(bf16[128,2048]{1,0:T(8,128)(2,1)} %reduce-scatter.3.cloned.1.call-done) | copy-start | bytes 1572868
Sparse Core Ops, SparseCore 0:
  57.5 30.8 reduce-scatter.2
  91.8 22.5 all-gather.4
  116.0 285.3 all-gather.6
  439.4 29.5 reduce-scatter.4
